TPU v7x, 128 devices: a whole 4x4x4 slice. The times are simulated.
128 devices in a mesh: sp: 32 (over z, y, core), tp: 4 (over x).
Axes of the slice: x: 4, y: 4, z: 4, core: 2. Of those that a mesh axis runs over, the one named last changes fastest.
Arguments:
- tokens: bfloat16 [32768, 2048], P('sp', 'tp'), may hold values from -6 to 6
- input_norm_gain: float32 [2048], replicated, may hold values from 0.1 to 1.9
- pooling_input_matrix: bfloat16 [2048, 512], P(None, 'tp'), may hold values from -0.125 to 0.125
- query_projection_matrix: bfloat16 [2048, 1024], P(None, 'tp'), may hold values from -0.125 to 0.125
- key_projection_matrix: bfloat16 [2048, 1024], P(None, 'tp'), may hold values from -0.125 to 0.125
- value_projection_matrix: bfloat16 [2048, 1024], P(None, 'tp'), may hold values from -0.125 to 0.125
- output_gate_matrix: bfloat16 [2048, 1024], P(None, 'tp'), may hold values from -0.125 to 0.125
- input_gate_matrix: bfloat16 [2048, 2, 8], replicated
- forget_gate_matrix: bfloat16 [2048, 2, 8], replicated, may hold values from -0.125 to 0.125
- forget_gate_bias: float32 [2, 8], replicated
- log_forget_scale: float32 [2, 32768], P(None, 'sp'), may hold values from 0.35 to 2.8
- extra_log_forget: float32 [2, 32768], P(None, 'sp'), may hold values from -0.7 to 0, as said below
- starting_memory: float32 [2, 8, 128, 128], P(None, 'tp'), may hold values from -3 to 3
- starting_normalizer: float32 [2, 8, 128], P(None, 'tp'), may hold values from -3 to 3
- starting_log_scale: float32 [2, 8], P(None, 'tp'), may hold values from 2 to 5
- pooling_group_map: bfloat16 [4, 128, 128], replicated, may hold values from -0.5 to 0.5
- pooling_channel_scale: float32 [512], replicated, may hold values from 0.1 to 1.9
- memory_head_gain: float32 [1024], replicated, may hold values from 0.1 to 1.9
- pooling_output_matrix: bfloat16 [512, 2048], replicated, may hold values from -0.25 to 0.25
- memory_output_matrix: bfloat16 [1024, 2048], replicated, may hold values from -0.1875 to 0.1875
Outputs:
- mixed_out: bfloat16 [32768, 2048], P(('sp', 'tp'))
Inputs may be any that keep to these rules, and one draw needn't show every extreme that they name: `extra_log_forget`: at most three nonzero entries in each direction.
All inputs are finite; a program needn't handle non-finite values.
Results may differ from a plain program's by a relative error of at most 0.0091.
Values may be sent and summed in bfloat16 or wider, within the bound.
A program may use at most 128 MiB of HBM per device.

v0:
```python
import jax
import jax.numpy as jnp
from jax import lax
from jax.sharding import PartitionSpec as P

DH = 128
BLOCK = 128
NEG_BIG = -1e30
LN_EPS = 1e-05
HEAD_EPS = 1e-06
RIM_ROWS = 8


def extended(block, sides, width):
    for axis, dim in sides:
        count = lax.axis_size(axis)
        forward = [(i, i + 1) for i in range(count - 1)]
        backward = [(target, source) for source, target in forward]
        low = lax.ppermute(
            lax.slice_in_dim(block, block.shape[dim] - width, None, axis=dim), axis, forward
        )
        high = lax.ppermute(lax.slice_in_dim(block, 0, width, axis=dim), axis, backward)
        block = jnp.concatenate([low, block, high], axis=dim)
    return block


def block_step(carried, pieces):
    memory, normer, maxlog = carried
    q_blk, k_blk, v_blk, i_blk, f_blk = pieces
    lower_mask = jnp.tril(jnp.ones((BLOCK, BLOCK), dtype=bool))
    cumulative = jnp.cumsum(f_blk, axis=-1)
    exponent = jnp.where(
        lower_mask, cumulative[:, :, None] - cumulative[:, None, :] + i_blk[:, None, :], NEG_BIG
    )
    carried_log = cumulative + maxlog[:, None]
    row_max = jnp.maximum(carried_log, exponent.max(-1))
    fading = jnp.exp(carried_log - row_max)
    scores = jnp.einsum("htd,hsd->hts", q_blk, k_blk) * jnp.exp(exponent - row_max[:, :, None])
    numerator = fading[:, :, None] * jnp.einsum("hvk,htk->htv", memory, q_blk) + jnp.einsum(
        "hts,hsv->htv", scores, v_blk
    )
    denominator = fading * jnp.einsum("hk,htk->ht", normer, q_blk) + scores.sum(-1)
    summed = cumulative[:, -1]
    weight_log = summed[:, None] - cumulative + i_blk
    new_max = jnp.maximum(summed + maxlog, weight_log.max(-1))
    carry_scale = jnp.exp(summed + maxlog - new_max)
    weights = jnp.exp(weight_log - new_max[:, None])
    memory = carry_scale[:, None, None] * memory + jnp.einsum(
        "hsv,hsk->hvk", v_blk * weights[:, :, None], k_blk
    )
    normer = carry_scale[:, None] * normer + jnp.einsum("hs,hsk->hk", weights, k_blk)
    return ((memory, normer, new_max), (numerator, denominator, row_max))


def to_blocks(source):
    return jnp.moveaxis(
        source.reshape((source.shape[0], source.shape[1] // BLOCK, BLOCK) + source.shape[2:]), 1, 0
    )


def from_blocks(source):
    return jnp.moveaxis(source, 0, 1).reshape(
        (source.shape[1], source.shape[0] * source.shape[2]) + source.shape[3:]
    )


def local_pass(query_heads, key_heads, value_heads, log_in, log_forget_gate):
    head_count = query_heads.shape[0]
    head_size = query_heads.shape[2]
    initial = (
        jnp.zeros((head_count, head_size, head_size), jnp.float32),
        jnp.zeros((head_count, head_size), jnp.float32),
        jnp.full((head_count,), NEG_BIG, jnp.float32),
    )
    finals, outputs = lax.scan(
        block_step,
        initial,
        tuple(
            (
                to_blocks(member)
                for member in (query_heads, key_heads, value_heads, log_in, log_forget_gate)
            )
        ),
    )
    numerator, denominator, row_max = (from_blocks(member) for member in outputs)
    falls = jnp.cumsum(log_forget_gate, axis=1)
    return ((falls[:, -1],) + finals, (numerator, denominator, row_max, falls))


def join_states(earlier, later):
    early_fall, early_memory, early_normer, early_max = earlier
    late_fall, late_memory, late_normer, late_max = later
    merged_max = jnp.maximum(early_max + late_fall, late_max)
    early_weight = jnp.exp(early_max + late_fall - merged_max)
    late_weight = jnp.exp(late_max - merged_max)
    return (
        late_fall,
        early_weight[..., None, None] * early_memory + late_weight[..., None, None] * late_memory,
        early_weight[..., None] * early_normer + late_weight[..., None] * late_normer,
        merged_max,
    )


def prefix_from_all(gathered, position, from_later):
    falls, memories, normers, maxima = gathered
    order = jnp.arange(falls.shape[0], dtype=jnp.int32)
    inclusive = jnp.cumsum(falls, axis=0)
    exclusive = inclusive - falls
    if from_later:
        valid = order > position
        between = exclusive - inclusive[position][None]
        total_fall = inclusive[-1] - inclusive[position]
    else:
        valid = order < position
        between = exclusive[position][None] - inclusive
        total_fall = exclusive[position]
    log_weight = jnp.where(valid[:, None], maxima + between, NEG_BIG)
    joint_max = jnp.max(log_weight, axis=0)
    weights = jnp.where(valid[:, None], jnp.exp(log_weight - joint_max[None]), 0.0)
    memory = jnp.einsum("jh,jhvk->hvk", weights, memories)
    normer = jnp.einsum("jh,jhk->hk", weights, normers)
    return (total_fall, memory, normer, joint_max)


def finish(local_terms, entering, query_heads):
    numerator, denominator, row_max, falls = local_terms
    fall_in, memory, normer, max_in = entering
    state_log = falls + max_in[:, None]
    joint_max = jnp.maximum(row_max, state_log)
    local_weight = jnp.exp(row_max - joint_max)
    state_weight = jnp.exp(state_log - joint_max)
    full_numerator = local_weight[..., None] * numerator + state_weight[..., None] * jnp.einsum(
        "hvk,htk->htv", memory, query_heads
    )
    full_denominator = local_weight * denominator + state_weight * jnp.einsum(
        "hk,htk->ht", normer, query_heads
    )
    return full_numerator / jnp.maximum(jnp.abs(full_denominator), 1.0)[..., None]


def per_device(
    tokens,
    input_norm_gain,
    pooling_input_matrix,
    query_projection_matrix,
    key_projection_matrix,
    value_projection_matrix,
    output_gate_matrix,
    input_gate_matrix,
    forget_gate_matrix,
    forget_gate_bias,
    log_forget_scale,
    extra_log_forget,
    starting_memory,
    starting_normalizer,
    starting_log_scale,
    pooling_group_map,
    pooling_channel_scale,
    memory_head_gain,
    pooling_output_matrix,
    memory_output_matrix,
):
    local_rows = tokens.shape[0]
    own_width = tokens.shape[1]
    model_width = own_width * lax.axis_size("tp")
    group_index = lax.axis_index("tp")
    seq_index = lax.axis_index("sp")
    group_dim = pooling_input_matrix.shape[1]
    head_local = query_projection_matrix.shape[1] // DH
    mem_width = head_local * DH
    main_weight = jnp.concatenate(
        [
            pooling_input_matrix,
            query_projection_matrix,
            key_projection_matrix,
            value_projection_matrix,
            output_gate_matrix,
        ],
        axis=1,
    )
    gate_in = lax.dynamic_slice_in_dim(input_gate_matrix, group_index * head_local, head_local, 2)
    gate_fg = lax.dynamic_slice_in_dim(forget_gate_matrix, group_index * head_local, head_local, 2)
    gate_weight = jnp.concatenate([gate_in, gate_fg], axis=1).reshape(model_width, 4 * head_local)
    whole_rows = lax.all_gather(tokens, "tp", axis=1, tiled=True)
    floats = whole_rows.astype(jnp.float32)
    mean_row = jnp.sum(floats, axis=1) / model_width
    variance = jnp.sum(floats * floats, axis=1) / model_width - mean_row * mean_row
    normed = (
        (floats - mean_row[:, None]) * lax.rsqrt(variance + LN_EPS)[:, None] * input_norm_gain
    ).astype(jnp.bfloat16)
    projected = jnp.dot(normed, main_weight, preferred_element_type=jnp.float32)
    gate_pre = jnp.dot(normed, gate_weight, preferred_element_type=jnp.float32)
    pool_in = projected[:, :group_dim].astype(jnp.bfloat16)
    queries = projected[:, group_dim : group_dim + mem_width].astype(jnp.bfloat16)
    key_rows = projected[:, group_dim + mem_width : group_dim + 2 * mem_width].astype(jnp.bfloat16)
    value_rows = projected[:, group_dim + 2 * mem_width : group_dim + 3 * mem_width].astype(
        jnp.bfloat16
    )
    out_gate = projected[:, group_dim + 3 * mem_width :].astype(jnp.bfloat16)
    gate_pre = gate_pre.reshape(local_rows, 2, 2, head_local)
    log_in = gate_pre[:, 0]
    bias_own = lax.dynamic_slice_in_dim(forget_gate_bias, group_index * head_local, head_local, 1)
    log_forget_gate = (
        jax.nn.log_sigmoid(gate_pre[:, 1] + bias_own[None]) * log_forget_scale.T[:, :, None]
        + extra_log_forget.T[:, :, None]
    )

    def heads_of(source, factor):
        return (
            (source.astype(jnp.float32) * factor)
            .reshape(local_rows, head_local, DH)
            .transpose(1, 0, 2)
        )

    query_heads = heads_of(queries, 1.0)
    key_heads = heads_of(key_rows, DH ** (-0.5))
    value_heads = heads_of(value_rows, 1.0)
    forward_summary, forward_local = local_pass(
        query_heads, key_heads, value_heads, log_in[:, 0].T, log_forget_gate[:, 0].T
    )
    flipped_query = query_heads[:, ::-1]
    backward_summary, backward_local = local_pass(
        flipped_query,
        key_heads[:, ::-1],
        value_heads[:, ::-1],
        log_in[:, 1].T[:, ::-1],
        log_forget_gate[:, 1].T[:, ::-1],
    )
    rimmed = extended(pool_in, (("sp", 0),), RIM_ROWS).astype(jnp.float32)
    half_span = jnp.left_shift(jnp.int32(1), group_index)
    grouped = pool_in.astype(jnp.float32)
    pooled = jnp.zeros_like(grouped)
    for offset in range(-RIM_ROWS, RIM_ROWS):
        inside = ((offset >= -half_span) & (offset < half_span)).astype(jnp.float32)
        pooled = pooled + inside * rimmed[RIM_ROWS + offset : RIM_ROWS + offset + local_rows]
    positions = seq_index * local_rows + jnp.arange(local_rows, dtype=jnp.int32)
    total_rows = local_rows * lax.axis_size("sp")
    counts = (
        jnp.minimum(positions + half_span, total_rows) - jnp.maximum(positions - half_span, 0)
    ).astype(jnp.float32)
    contrast = (pooled / counts[:, None] - grouped).astype(jnp.bfloat16)
    map_own = lax.dynamic_index_in_dim(pooling_group_map, group_index, 0, keepdims=False)
    scale_own = lax.dynamic_slice_in_dim(
        pooling_channel_scale, group_index * group_dim, group_dim, 0
    )
    pool_out = (jnp.dot(contrast, map_own, preferred_element_type=jnp.float32) * scale_own).astype(
        jnp.bfloat16
    )
    stacked = tuple(
        (
            jnp.stack([forward_part, backward_part])[None]
            for forward_part, backward_part in zip(forward_summary, backward_summary)
        )
    )
    gathered = lax.all_gather(stacked, "sp", axis=0, tiled=True)
    forward_prefix = prefix_from_all(tuple((member[:, 0] for member in gathered)), seq_index, False)
    backward_prefix = prefix_from_all(tuple((member[:, 1] for member in gathered)), seq_index, True)

    def initial_state(direction):
        return (
            jnp.zeros((head_local,), jnp.float32),
            starting_memory[direction],
            starting_normalizer[direction],
            starting_log_scale[direction],
        )

    forward = finish(forward_local, join_states(initial_state(0), forward_prefix), query_heads)
    backward = finish(backward_local, join_states(initial_state(1), backward_prefix), flipped_query)
    hidden = forward + backward[:, ::-1]
    head_mean = jnp.mean(hidden, axis=-1, keepdims=True)
    head_var = jnp.mean(jnp.square(hidden - head_mean), axis=-1, keepdims=True)
    gain_heads = lax.dynamic_slice_in_dim(
        memory_head_gain, group_index * mem_width, mem_width, 0
    ).reshape(head_local, DH)
    scaled = (hidden - head_mean) * lax.rsqrt(head_var + HEAD_EPS) * gain_heads[:, None, :]
    mem_out = (
        scaled.transpose(1, 0, 2).reshape(local_rows, mem_width)
        * jax.nn.sigmoid(out_gate.astype(jnp.float32))
    ).astype(jnp.bfloat16)
    mixed = jnp.concatenate([pool_out, mem_out], axis=1)
    owned = lax.all_to_all(mixed, "tp", split_axis=0, concat_axis=1, tiled=True)
    owner_rows = owned.shape[0]
    owned = owned.reshape(owner_rows, lax.axis_size("tp"), group_dim + mem_width)
    pool_part = owned[:, :, :group_dim].reshape(owner_rows, lax.axis_size("tp") * group_dim)
    mem_part = owned[:, :, group_dim:].reshape(owner_rows, lax.axis_size("tp") * mem_width)
    result = jnp.dot(
        pool_part, pooling_output_matrix, preferred_element_type=jnp.float32
    ) + jnp.dot(mem_part, memory_output_matrix, preferred_element_type=jnp.float32)
    return result.astype(jnp.bfloat16)


def solution(mesh):
    placed = (
        P("sp", "tp"),
        P(),
        P(None, "tp"),
        P(None, "tp"),
        P(None, "tp"),
        P(None, "tp"),
        P(None, "tp"),
        P(),
        P(),
        P(),
        P(None, "sp"),
        P(None, "sp"),
        P(None, "tp", None, None),
        P(None, "tp", None),
        P(None, "tp"),
        P(),
        P(),
        P(),
        P(),
        P(),
    )
    return jax.shard_map(
        per_device, mesh=mesh, in_specs=placed, out_specs=P(("sp", "tp"), None), check_vma=False
    )
```

profile of v0, /device:TPU:1, one launch (start us, length us, event | category | flops | bytes accessed | tf_op | source)
XLA Modules:
  0.0 383.7 jit_solution(3305362146877481871)
XLA Ops:
  9.4 1.9 constant_dynamic-update-slice_fusion.8
  11.3 2.3 constant_dynamic-update-slice_fusion.7
  16.9 43.3 %all-gather.9.cloned.1.call-done = bf16[1024,2048]{1,0:T(8,128)(2,1)} async-done(((bf16[1024,512]{1,0:T(8,128)(2,1)}), bf16[1024,2048]{1,0:T(8,128)(2,1)}) %all-gather.9.cloned.1.call-update) | async-done | bytes 4194320 | tf_op jit(solution)/shard_map/all_gather | solution.py:184
  60.2 3.6 convert_reduce_fusion
  63.9 8.5 %convolution_convert_fusion = bf16[1024,1152]{1,0:T(8,128)(2,1)S(1)} fusion(bf16[2048,1152]{1,0:T(8,128)(2,1)} %constant_dynamic-update-slice_fusion.4, bf16[1024,2048]{1,0:T(8,128)(2,1)S(1)} %copy-done.5, f32[2048]{0:T(1024)S(1)} %copy-done.21, f32[1024]{0:T(1024)S(1)} %get-tuple-element.398, f32[1024]{0:T(1024)S(1)} %get-tuple-element.397), kind=kOutput, calls=%fused_computation.125 | convolution fusion | flops 4843503616 | bytes 11288576 | tf_op jit(solution)/shard_map/dot_general | solution.py:191
  72.4 1.5 multiply_bitcast_fusion
  74.7 1.3 copy_bitcast_fusion
  75.9 5.1 %rev.22 = bf16[2,1024,128]{2,1,0:T(8,128)(2,1)} reverse(bf16[2,1024,128]{2,1,0:T(8,128)(2,1)S(1)} %get-tuple-element.407), dimensions={1} | reverse | bytes 1048576 | tf_op jit(solution)/shard_map/rev | solution.py:221
  81.0 3.7 fusion.70
  86.3 1.3 copy.211
  87.6 5.1 %rev.20 = f32[2,1024,128]{2,1,0:T(8,128)} reverse(f32[2,1024,128]{2,1,0:T(8,128)S(1)} %bitcast.498), dimensions={1} | reverse | bytes 2097152 | tf_op jit(solution)/shard_map/rev | solution.py:225
  92.7 8.2 %rev.21 = bf16[2,1024,128]{2,1,0:T(8,128)(2,1)} reverse(bf16[2,1024,128]{2,1,0:T(8,128)(2,1)} %get-tuple-element.381), dimensions={1} | reverse | bytes 1048576 | tf_op jit(solution)/shard_map/rev | solution.py:224
  101.0 1.9 copy.212
  104.0 66.0 %while.43 = (s32[]{:T(128)}, f32[2,128,128]{2,1,0:T(8,128)S(1)}, f32[2,128]{1,0:T(2,128)S(1)}, f32[2]{0:T(128)S(1)}, f32[8,2,128,128]{3,2,1,0:T(8,128)}, /*index...) while((s32[]{:T(128)}, f32[2,128,128]{2,1,0:T(8,128)S(1)}, ...), condition=%wide.region_18.19_spmd.clone, body=%wide.region_13.18_spmd.clone.sunk | while | flops 34327816 | bytes 1600317 | solution.py:75
  110.4 1.8 fusion.266
  118.7 1.8 fusion.266
  126.9 1.8 fusion.266
  135.1 1.8 fusion.266
  143.4 1.8 fusion.266
  151.6 1.8 fusion.266
  159.9 1.8 fusion.266
  168.1 1.8 fusion.266
  169.9 1.9 copy.213
  172.9 58.1 %while.42 = (s32[]{:T(128)}, f32[2,128,128]{2,1,0:T(8,128)S(1)}, f32[2,128]{1,0:T(2,128)S(1)}, f32[2]{0:T(128)S(1)}, f32[8,2,128,128]{3,2,1,0:T(8,128)}, /*index...) while((s32[]{:T(128)}, f32[2,128,128]{2,1,0:T(8,128)S(1)}, ...), condition=%wide.region_7.8_spmd.clone, body=%wide.region_2.7_spmd.clone.sunk | while | flops 34327816 | bytes 1600821 | solution.py:75
  231.8 1.3 dynamic_slice.60
  236.3 25.2 %all-gather.4 = f32[32,2,2]{2,1,0:T(2,128)S(1)} all-gather(f32[1,2,2]{2,1,0:T(2,128)S(1)} %maximum_bitcast_fusion), channel_id=2, replica_groups=mesh['sp'=32,'tp'=4] {'sp'}, dimensions={0}, use_global_device_ids=true | all-gather | bytes 528 | tf_op jit(solution)/shard_map/all_gather | solution.py:255
  261.7 23.6 %all-gather.5 = f32[32,2,2]{2,1,0:T(2,128)S(1)} all-gather(f32[1,2,2]{2,1,0:T(2,128)S(1)} %maximum_bitcast_fusion.1), channel_id=3, replica_groups=mesh['sp'=32,'tp'=4] {'sp'}, dimensions={0}, use_global_device_ids=true | all-gather | bytes 528 | tf_op jit(solution)/shard_map/all_gather | solution.py:255
  286.8 2.1 collective-permute-start.1
  288.9 3.5 collective-permute-start
  292.4 22.6 %all-gather.3 = bf16[64,2,128]{2,1,0:T(2,128)(2,1)S(1)} all-gather(bf16[2,2,128]{2,1,0:T(2,128)(2,1)S(1)} %pad_maximum_fusion.3), channel_id=5, replica_groups=mesh['sp'=32,'tp'=4] {'sp'}, dimensions={0}, use_global_device_ids=true | all-gather | bytes 33792 | tf_op jit(solution)/shard_map/all_gather | solution.py:255
  315.6 1.3 fusion.177
  317.0 1.3 fusion.83
  318.4 2.6 copy.115
  321.0 2.4 reshape.649
  323.6 1.3 copy.109
  324.9 2.4 reshape.646
  327.4 2.1 fusion.82
  329.5 4.2 %slice_bitcast_fusion.1 = (bf16[32,2,128,128]{3,2,1,0:T(8,128)(2,1)}, bf16[32,2,128,128]{3,2,1,0:T(8,128)(2,1)S(1)}) fusion(bf16[32,2,2,128,128]{4,3,2,1,0:T(8,128)(2,1)} %bitcast.502), kind=kLoop, calls=%fused_computation.118 | loop fusion | bytes 8388608 | tf_op jit(solution)/shard_map/squeeze | solution.py:256
  333.7 1.2 fusion.72
  335.0 1.3 fusion.81
  336.4 9.4 %rev.23 = f32[2,1024,128]{1,2,0:T(8,128)} reverse(f32[2,1024,128]{1,2,0:T(8,128)} %fusion.81), dimensions={1} | reverse | bytes 2097152 | tf_op jit(solution)/shard_map/rev | solution.py:269
  345.7 2.8 fusion.74
  348.6 2.0 fusion.176
  351.9 1.6 copy.152
  353.4 1.3 multiply_convert_fusion
  356.0 15.5 %all_to_all.16 = bf16[4,256,384]{1,2,0:T(8,128)(2,1)S(1)} all-to-all(bf16[4,256,384]{1,2,0:T(8,128)(2,1)} %copy.118), channel_id=1, replica_groups=mesh['sp'=32,'tp'=4] {'tp'}, dimensions={0} | all-to-all | bytes 1572864 | tf_op jit(solution)/shard_map/all_to_all | solution.py:281
  371.6 3.5 fusion.178
  375.1 1.7 fusion.76
  (422 shorter events, 128.8 us)
Async XLA Ops:
  6.5 368.6 %copy-start = (bf16[512,2048]{1,0:T(8,128)(2,1)S(1)}, bf16[512,2048]{1,0:T(8,128)(2,1)}, u32[]{:S(2)}) copy-start(bf16[512,2048]{1,0:T(8,128)(2,1)} %param.42) | copy-start | bytes 6291460
  6.5 7.1 %copy-start.8 = (bf16[2048,256]{1,0:T(8,128)(2,1)S(1)}, bf16[2048,256]{1,0:T(8,128)(2,1)}, u32[]{:S(2)}) copy-start(bf16[2048,256]{1,0:T(8,128)(2,1)} %param.28) | copy-start | bytes 3145732
  6.5 53.7 %all-gather.9.cloned.1.call-start = ((), (), s32[]{:S(2)}) async-start(), calls=%async_computation.1 | async-start | bytes 5242880 | tf_op jit(solution)/shard_map/all_gather | solution.py:184
  7.3 322.2 %all-gather.11.cloned.1.call-start = ((), (), s32[]{:S(2)}) async-start(), calls=%async_computation.2 | async-start | bytes 4325376 | tf_op jit(solution)/shard_map/all_gather | solution.py:255
  8.4 6.2 %copy-start.9 = (bf16[2048,256]{1,0:T(8,128)(2,1)S(1)}, bf16[2048,256]{1,0:T(8,128)(2,1)}, u32[]{:S(2)}) copy-start(bf16[2048,256]{1,0:T(8,128)(2,1)} %param.29) | copy-start | bytes 3145732
  8.5 7.3 %copy-start.10 = (bf16[2048,256]{1,0:T(8,128)(2,1)S(1)}, bf16[2048,256]{1,0:T(8,128)(2,1)}, u32[]{:S(2)}) copy-start(bf16[2048,256]{1,0:T(8,128)(2,1)} %param.30) | copy-start | bytes 3145732
  14.7 49.2 %copy-start.21 = (f32[2048]{0:T(1024)S(1)}, f32[2048]{0:T(1024)}, u32[]{:S(2)}) copy-start(f32[2048]{0:T(1024)} %param.25) | copy-start | bytes 24580
  60.2 3.6 copy-start.5
  72.4 3.5 copy-start.7
  73.9 0.8 copy-start.1
  75.9 8.8 %copy-start.3 = (bf16[2,1024,128]{2,1,0:T(8,128)(2,1)}, bf16[2,1024,128]{2,1,0:T(8,128)(2,1)S(1)}, u32[]{:S(2)}) copy-start(bf16[2,1024,128]{2,1,0:T(8,128)(2,1)S(1)} %get-tuple-element.407) | copy-start | bytes 1572868
  81.0 3.7 copy-start.12
  81.0 3.7 copy-start.13
  172.9 113.0 %copy-start.15 = (f32[2,2]{1,0:T(2,128)S(1)}, f32[2,2]{1,0:T(2,128)}, u32[]{:S(2)}) copy-start(f32[2,2]{1,0:T(2,128)} %param.38) | copy-start | bytes 52
  172.9 142.5 %copy-start.14 = (f32[2,2,128]{2,1,0:T(2,128)S(1)}, f32[2,2,128]{2,1,0:T(2,128)}, u32[]{:S(2)}) copy-start(f32[2,2,128]{2,1,0:T(2,128)} %param.37) | copy-start | bytes 6148
  231.0 92.6 %copy-start.6 = (f32[8,2,128,128]{3,2,1,0:T(8,128)S(1)}, f32[8,2,128,128]{3,2,1,0:T(8,128)}, u32[]{:S(2)}) copy-start(f32[8,2,128,128]{3,2,1,0:T(8,128)} %get-tuple-element.142) | copy-start | bytes 3145732
  286.8 40.5 %collective-permute-start.1 = (bf16[8,128]{1,0:T(8,128)(2,1)S(1)}, bf16[8,128]{1,0:T(8,128)(2,1)S(1)}, u32[]{:S(2)}, u32[]{:S(2)}) collective-permute-start(bf16[8,128]{1,0:T(8,128)(2,1)S(1)} %get-tuple-element.374), channel_id=1, source_target_pairs={{4,0},{8,4},{12,8},{16,12},{20,16},{24,20},{28,24},{32,28},{36,32}... | collective-permute-start | bytes 6152 | tf_op jit(solution)/shard_map/ppermute | solution.py:22
  288.9 38.4 %collective-permute-start = (bf16[8,128]{1,0:T(8,128)(2,1)S(1)}, bf16[8,128]{1,0:T(8,128)(2,1)S(1)}, u32[]{:S(2)}, u32[]{:S(2)}) collective-permute-start(bf16[8,128]{1,0:T(8,128)(2,1)S(1)} %get-tuple-element.373), channel_id=1, source_target_pairs={{0,4},{4,8},{8,12},{12,16},{16,20},{20,24},{24,28},{28,32},{32,36}... | collective-permute-start | bytes 6152 | tf_op jit(solution)/shard_map/ppermute | solution.py:19
  315.1 1.9 copy-start.16
  315.1 0.5 copy-start.18
  318.4 8.9 %slice-start = ((bf16[1024,1152]{1,0:T(8,128)(2,1)}), bf16[1024,128]{1,0:T(8,128)(2,1)S(1)}, s32[]{:S(2)}) async-start(bf16[1024,1152]{1,0:T(8,128)(2,1)} %copy-done.7), calls=%async_computation.3 | async-start | bytes 524288 | tf_op jit(solution)/shard_map/slice | solution.py:193
  318.4 8.9 %copy-start.22 = (f32[128]{0:T(128)S(1)}, f32[128]{0:T(128)}, u32[]{:S(2)}) copy-start(f32[128]{0:T(128)} %dynamic_slice.60) | copy-start | bytes 1540
  329.5 5.5 %copy-start.4 = (bf16[2,1024,128]{2,1,0:T(8,128)(2,1)S(1)}, bf16[2,1024,128]{2,1,0:T(8,128)(2,1)}, u32[]{:S(2)}) copy-start(bf16[2,1024,128]{2,1,0:T(8,128)(2,1)} %rev.22) | copy-start | bytes 1572868
  329.5 5.5 %copy-start.11 = (f32[2,1024,128]{1,2,0:T(8,128)S(1)}, f32[2,1024,128]{1,2,0:T(8,128)}, u32[]{:S(2)}) copy-start(f32[2,1024,128]{1,2,0:T(8,128)} %reshape.649) | copy-start | bytes 3145732
  329.5 5.5 %copy-start.19 = (f32[2]{0:T(128)S(1)}, f32[2]{0:T(128)}, u32[]{:S(2)}) copy-start(f32[2]{0:T(128)} %copy-done.18) | copy-start | bytes 28
  329.5 5.5 %copy-start.20 = (f32[2,2,128,128]{3,2,1,0:T(8,128)S(1)}, f32[2,2,128,128]{3,2,1,0:T(8,128)}, u32[]{:S(2)}) copy-start(f32[2,2,128,128]{3,2,1,0:T(8,128)} %param.36) | copy-start | bytes 786436
  335.0 13.6 %copy-start.2 = (bf16[128,2,8,128]{3,2,1,0:T(8,128)(2,1)S(1)}, bf16[128,2,8,128]{3,2,1,0:T(8,128)(2,1)}, u32[]{:S(2)}) copy-start(bf16[128,2,8,128]{3,2,1,0:T(8,128)(2,1)} %copy-done.1) | copy-start | bytes 1572868
  335.0 13.6 %copy-start.17 = (f32[2]{0:T(128)S(1)}, f32[2]{0:T(128)}, u32[]{:S(2)}) copy-start(f32[2]{0:T(128)} %copy-done.16) | copy-start | bytes 28
Sparse Core Ops, SparseCore 0:
  9.0 51.1 all-gather.8
  231.8 47.1 all-gather.10
where the time goes:
time: 390 us; the launch traced here: 384 us
  matrix products  134 us (34%)
  blocking collectives  86.9 us (22%)
  local copies, waits for them, and re-layouts  71.2 us (18%)
  waiting for transfers between devices  44.1 us (11%)
  other arithmetic  26.8 us (7%)
  between operations  14 us (4%)
  starting transfers between devices  5.59 us (1%)
    all_gather x3, blocking collectives, per_device(): gathered = lax.all_gather(stacked, 'sp', axis=0, tiled=True)  71.4 us
    all_gather x1, waiting for transfers between devices, per_device(): whole_rows = lax.all_gather(tokens, 'tp', axis=1, tiled=True)  43.3 us
    dot_general x16, matrix products, block_step(): jnp.einsum('hts,hsv->htv', scores, v_blk)  21.4 us
    dot_general x16, matrix products, block_step(): jnp.einsum('hsv,hsk->hvk', v_blk * weights[:, :, None], k_blk)  18.7 us
    dot_general x16, matrix products, block_step(): jnp.einsum('htd,hsd->hts', q_blk, k_blk)  16.9 us
    dot_general x16, matrix products, block_step(): jnp.einsum('hvk,htk->htv', memory, q_blk)  16.6 us
    dot_general x16, matrix products, block_step(): jnp.einsum('hk,htk->ht', normer, q_blk)  15.5 us
    all_to_all x1, blocking collectives, per_device(): owned = lax.all_to_all(mixed, 'tp', split_axis=0, concat_axis=1, tiled=True)  15.5 us
  transfers between devices with their start and end apart: 4, of which 1 were waited for; matrix products, arithmetic and copies ran while one was open for 8% of the time, Pallas kernels for 0%

commit v1 on v0

--- a/solution.py
+++ b/solution.py
@@ -181,7 +181,8 @@
     gate_in = lax.dynamic_slice_in_dim(input_gate_matrix, group_index * head_local, head_local, 2)
     gate_fg = lax.dynamic_slice_in_dim(forget_gate_matrix, group_index * head_local, head_local, 2)
     gate_weight = jnp.concatenate([gate_in, gate_fg], axis=1).reshape(model_width, 4 * head_local)
-    whole_rows = lax.all_gather(tokens, "tp", axis=1, tiled=True)
+    _cut_cards = lambda own_rows, chip_axis: jnp.concatenate(lax.all_gather(own_rows, chip_axis), 1)
+    whole_rows = _cut_cards(tokens, chip_axis="tp")
     floats = whole_rows.astype(jnp.float32)
     mean_row = jnp.sum(floats, axis=1) / model_width
     variance = jnp.sum(floats * floats, axis=1) / model_width - mean_row * mean_row

time: 390 us -> 416 us (1.067)
  local copies, waits for them, and re-layouts: 71.2 us -> 86.8 us
  other arithmetic: 26.8 us -> 36.5 us
    convert_element_type x0 -> x2, local copies, waits for them, and re-layouts: none -> 15.1 us  [the longest x1 8.75 us: per_device(): floats = whole_rows.astype(jnp.float32)]
    convert_element_type x0 -> x3, other arithmetic: none -> 12 us  [the longest x2 8.67 us: per_device(): normed = ((floats - mean_row[:, None]) * lax.rsqrt(variance + LN_EPS)[:,...]
    unnamed x57 -> x55, local copies, waits for them, and re-layouts: 7.71 us -> 12.9 us
    rev x1, local copies, waits for them, and re-layouts: 5.08 us -> 0.54 us  [per_device(): flipped_query = query_heads[:, ::-1]]
  transfers between devices with their start and end apart: 4 -> 4, of which waited for: 1 -> 1; matrix products, arithmetic and copies ran while one was open for 8% -> 7% of each run, Pallas kernels for 0% -> 0%
where the time goes in v1:
time: 416 us; the launch traced here: 410 us
  matrix products  134 us (32%)
  blocking collectives  88.1 us (21%)
  local copies, waits for them, and re-layouts  86.8 us (21%)
  waiting for transfers between devices  43.4 us (10%)
  other arithmetic  36.5 us (9%)
  between operations  14 us (3%)
  starting transfers between devices  5.97 us (1%)
    all_gather x3, blocking collectives, per_device(): gathered = lax.all_gather(stacked, 'sp', axis=0, tiled=True)  72.5 us
    all_gather x1, waiting for transfers between devices, per_device(): lax.all_gather(own_rows, chip_axis)  42.6 us
    dot_general x16, matrix products, block_step(): jnp.einsum('hts,hsv->htv', scores, v_blk)  21.3 us
    dot_general x16, matrix products, block_step(): jnp.einsum('hsv,hsk->hvk', v_blk * weights[:, :, None], k_blk)  18.6 us
    dot_general x16, matrix products, block_step(): jnp.einsum('htd,hsd->hts', q_blk, k_blk)  16.9 us
    dot_general x16, matrix products, block_step(): jnp.einsum('hvk,htk->htv', memory, q_blk)  16.6 us
    all_to_all x1, blocking collectives, per_device(): owned = lax.all_to_all(mixed, 'tp', split_axis=0, concat_axis=1, tiled=True)  15.5 us
    dot_general x16, matrix products, block_step(): jnp.einsum('hk,htk->ht', normer, q_blk)  15.5 us
  transfers between devices with their start and end apart: 4, of which 1 were waited for; matrix products, arithmetic and copies ran while one was open for 7% of the time, Pallas kernels for 0%

profile of v1, /device:TPU:1, one launch (start us, length us, event | category | flops | bytes accessed | tf_op | source)
XLA Modules:
  0.0 409.6 jit_solution(14835070516339681995)
XLA Ops:
  10.1 2.0 constant_dynamic-update-slice_fusion.8
  12.0 2.3 constant_dynamic-update-slice_fusion.7
  17.6 42.6 %all-gather.10.cloned.1.call-done = bf16[4096,512]{1,0:T(8,128)(2,1)} async-done(((bf16[1024,512]{1,0:T(8,128)(2,1)}), bf16[4096,512]{1,0:T(8,128)(2,1)}) %all-gather.10.cloned.1.call-update) | async-done | bytes 4194320 | tf_op jit(solution)/shard_map/all_gather | solution.py:184
  60.2 3.4 convert_element_type.145
  64.3 3.6 copy-done.1
  69.5 8.8 %copy.202 = f32[1024,4,512]{0,2,1:T(8,128)} copy(f32[1024,4,512]{2,0,1:T(8,128)} %bitcast.511) | data formatting | bytes 16777216 | tf_op jit(solution)/shard_map/convert_element_type | solution.py:186
  78.3 5.4 %fusion.68 = bf16[1024,2048]{0,1:T(8,128)(2,1)} fusion(f32[1024,4,512]{0,2,1:T(8,128)} %copy.202, f32[2048]{0:T(1024)S(1)} %copy-done.15, f32[1024]{0:T(1024)S(1)} %get-tuple-element.468, f32[1024]{0:T(1024)S(1)} %get-tuple-element.467), kind=kLoop, calls=%fused_computation.113 | loop fusion | flops 8388608 | bytes 12599296 | tf_op jit(solution)/shard_map/convert_element_type | solution.py:191
  84.4 3.3 fusion.69
  87.7 6.3 %copy.204 = bf16[1024,4,512]{0,2,1:T(8,128)(2,1)} copy(bf16[1024,4,512]{2,0,1:T(8,128)(2,1)} %fusion.69) | data formatting | bytes 8388608 | tf_op jit(solution)/shard_map/convert_element_type | solution.py:191
  94.0 3.0 fusion.173
  98.6 8.9 %convolution_convert_fusion = bf16[1024,1152]{1,0:T(8,128)(2,1)S(1)} fusion(bf16[1024,2048]{0,1:T(8,128)(2,1)} %fusion.68, bf16[2048,1152]{1,0:T(8,128)(2,1)} %constant_dynamic-update-slice_fusion.4), kind=kOutput, calls=%fused_computation.123 | convolution fusion | flops 4833017856 | bytes 11272192 | tf_op jit(solution)/shard_map/dot_general | solution.py:192
  107.5 1.5 multiply_bitcast_fusion
  112.5 8.2 %rev.21 = bf16[2,1024,128]{2,1,0:T(8,128)(2,1)} reverse(bf16[2,1024,128]{2,1,0:T(8,128)(2,1)} %get-tuple-element.451), dimensions={1} | reverse | bytes 1048576 | tf_op jit(solution)/shard_map/rev | solution.py:225
  120.8 1.3 copy.329
  122.1 5.1 %rev.20 = f32[2,1024,128]{2,1,0:T(8,128)} reverse(f32[2,1024,128]{2,1,0:T(8,128)S(1)} %bitcast.514), dimensions={1} | reverse | bytes 2097152 | tf_op jit(solution)/shard_map/rev | solution.py:226
  128.2 66.1 %while.43 = (s32[]{:T(128)}, f32[2,128,128]{2,1,0:T(8,128)S(1)}, f32[2,128]{1,0:T(2,128)S(1)}, f32[2]{0:T(128)S(1)}, f32[8,2,128,128]{3,2,1,0:T(8,128)}, /*index...) while((s32[]{:T(128)}, f32[2,128,128]{2,1,0:T(8,128)S(1)}, ...), condition=%wide.region_18.19_spmd.clone, body=%wide.region_13.18_spmd.clone.sunk | while | flops 34327816 | bytes 1601322 | solution.py:75
  133.5 1.8 fusion.265
  141.7 1.8 fusion.265
  150.0 1.8 fusion.265
  158.3 1.8 fusion.265
  166.5 1.8 fusion.265
  174.8 1.8 fusion.265
  183.0 1.8 fusion.265
  191.3 1.8 fusion.265
  194.3 1.9 copy.331
  197.4 58.2 %while.42 = (s32[]{:T(128)}, f32[2,128,128]{2,1,0:T(8,128)S(1)}, f32[2,128]{1,0:T(2,128)S(1)}, f32[2]{0:T(128)S(1)}, f32[8,2,128,128]{3,2,1,0:T(8,128)}, /*index...) while((s32[]{:T(128)}, f32[2,128,128]{2,1,0:T(8,128)S(1)}, ...), condition=%wide.region_7.8_spmd.clone, body=%wide.region_2.7_spmd.clone.sunk | while | flops 34327816 | bytes 1601826 | solution.py:75
  259.1 3.8 collective-permute-start
  263.0 2.1 collective-permute-start.1
  267.5 26.9 %all-gather.5 = f32[32,2,2]{2,1,0:T(2,128)S(1)} all-gather(f32[1,2,2]{2,1,0:T(2,128)S(1)} %maximum_bitcast_fusion), channel_id=3, replica_groups=mesh['sp'=32,'tp'=4] {'sp'}, dimensions={0}, use_global_device_ids=true | all-gather | bytes 528 | tf_op jit(solution)/shard_map/all_gather | solution.py:256
  294.8 21.8 %all-gather.6 = f32[32,2,2]{2,1,0:T(2,128)S(1)} all-gather(f32[1,2,2]{2,1,0:T(2,128)S(1)} %maximum_bitcast_fusion.1), channel_id=4, replica_groups=mesh['sp'=32,'tp'=4] {'sp'}, dimensions={0}, use_global_device_ids=true | all-gather | bytes 528 | tf_op jit(solution)/shard_map/all_gather | solution.py:256
  317.3 23.8 %all-gather.4 = bf16[64,2,128]{2,1,0:T(2,128)(2,1)S(1)} all-gather(bf16[2,2,128]{2,1,0:T(2,128)(2,1)S(1)} %pad_maximum_fusion.3), channel_id=6, replica_groups=mesh['sp'=32,'tp'=4] {'sp'}, dimensions={0}, use_global_device_ids=true | all-gather | bytes 33792 | tf_op jit(solution)/shard_map/all_gather | solution.py:256
  341.5 1.3 fusion.81
  342.9 1.3 fusion.174
  344.4 2.6 copy.232
  347.1 2.4 reshape.668
  349.4 1.3 copy.226
  350.8 2.4 reshape.665
  353.3 2.1 fusion.80
  355.4 4.2 %slice_bitcast_fusion.1 = (bf16[32,2,128,128]{3,2,1,0:T(8,128)(2,1)}, bf16[32,2,128,128]{3,2,1,0:T(8,128)(2,1)S(1)}) fusion(bf16[32,2,2,128,128]{4,3,2,1,0:T(8,128)(2,1)} %bitcast.518), kind=kLoop, calls=%fused_computation.118 | loop fusion | bytes 8388608 | tf_op jit(solution)/shard_map/squeeze | solution.py:257
  360.9 1.3 fusion.79
  362.3 9.4 %rev.23 = f32[2,1024,128]{1,2,0:T(8,128)} reverse(f32[2,1024,128]{1,2,0:T(8,128)} %fusion.79), dimensions={1} | reverse | bytes 2097152 | tf_op jit(solution)/shard_map/rev | solution.py:270
  371.7 2.8 fusion.72
  374.5 2.0 fusion.172
  377.8 1.6 copy.270
  379.3 1.3 multiply_convert_fusion.1
  381.9 15.5 %all_to_all.16 = bf16[4,256,384]{1,2,0:T(8,128)(2,1)S(1)} all-to-all(bf16[4,256,384]{1,2,0:T(8,128)(2,1)} %copy.235), channel_id=1, replica_groups=mesh['sp'=32,'tp'=4] {'tp'}, dimensions={0} | all-to-all | bytes 1572864 | tf_op jit(solution)/shard_map/all_to_all | solution.py:282
  397.5 3.5 fusion.175
  401.0 1.7 fusion.74
  (429 shorter events, 137.4 us)
Async XLA Ops:
  6.5 394.5 %copy-start = (bf16[512,2048]{1,0:T(8,128)(2,1)S(1)}, bf16[512,2048]{1,0:T(8,128)(2,1)}, u32[]{:S(2)}) copy-start(bf16[512,2048]{1,0:T(8,128)(2,1)} %param.42) | copy-start | bytes 6291460
  6.5 7.8 %copy-start.11 = (bf16[2048,256]{1,0:T(8,128)(2,1)S(1)}, bf16[2048,256]{1,0:T(8,128)(2,1)}, u32[]{:S(2)}) copy-start(bf16[2048,256]{1,0:T(8,128)(2,1)} %param.28) | copy-start | bytes 3145732
  6.5 53.7 %all-gather.10.cloned.1.call-start = ((), (), s32[]{:S(2)}) async-start(), calls=%async_computation.1 | async-start | bytes 5242880 | tf_op jit(solution)/shard_map/all_gather | solution.py:184
  7.3 348.1 %all-gather.12.cloned.1.call-start = ((), (), s32[]{:S(2)}) async-start(), calls=%async_computation.2 | async-start | bytes 4325376 | tf_op jit(solution)/shard_map/all_gather | solution.py:256
  9.1 6.3 %copy-start.12 = (bf16[2048,256]{1,0:T(8,128)(2,1)S(1)}, bf16[2048,256]{1,0:T(8,128)(2,1)}, u32[]{:S(2)}) copy-start(bf16[2048,256]{1,0:T(8,128)(2,1)} %param.29) | copy-start | bytes 3145732
  9.2 7.4 %copy-start.13 = (bf16[2048,256]{1,0:T(8,128)(2,1)S(1)}, bf16[2048,256]{1,0:T(8,128)(2,1)}, u32[]{:S(2)}) copy-start(bf16[2048,256]{1,0:T(8,128)(2,1)} %param.30) | copy-start | bytes 3145732
  63.6 4.3 %copy-start.1 = (f32[4096,512]{1,0:T(8,128)}, f32[4096,512]{1,0:T(8,128)S(1)}, u32[]{:S(2)}) copy-start(f32[4096,512]{1,0:T(8,128)S(1)} %convert_element_type.145) | copy-start | bytes 25165828
  63.6 5.2 %copy-start.2 = (bf16[4096,512]{1,0:T(8,128)(2,1)S(1)}, bf16[4096,512]{1,0:T(8,128)(2,1)}, u32[]{:S(2)}) copy-start(bf16[4096,512]{1,0:T(8,128)(2,1)} %all-gather.10.cloned.1.call-done) | copy-start | bytes 12582916
  69.5 8.8 %copy-start.15 = (f32[2048]{0:T(1024)S(1)}, f32[2048]{0:T(1024)}, u32[]{:S(2)}) copy-start(f32[2048]{0:T(1024)} %param.25) | copy-start | bytes 24580
  78.3 6.2 %copy-start.3 = (bf16[4096,512]{1,0:T(8,128)(2,1)S(1)}, bf16[4096,512]{1,0:T(8,128)(2,1)}, u32[]{:S(2)}) copy-start(bf16[4096,512]{1,0:T(8,128)(2,1)} %all-gather.10.cloned.1.call-done) | copy-start | bytes 12582916
  94.0 3.0 copy-start.16
  94.0 3.0 copy-start.17
  107.5 3.5 copy-start.10
  109.0 0.8 copy-start.4
  111.0 9.7 %copy-start.6 = (bf16[2,1024,128]{2,1,0:T(8,128)(2,1)}, bf16[2,1024,128]{2,1,0:T(8,128)(2,1)S(1)}, u32[]{:S(2)}) copy-start(bf16[2,1024,128]{2,1,0:T(8,128)(2,1)S(1)} %get-tuple-element.477) | copy-start | bytes 1572868
  111.6 9.2 %copy-start.7 = (bf16[2,1024,128]{2,1,0:T(8,128)(2,1)}, bf16[2,1024,128]{2,1,0:T(8,128)(2,1)S(1)}, u32[]{:S(2)}) copy-start(bf16[2,1024,128]{2,1,0:T(8,128)(2,1)S(1)} %rev.22) | copy-start | bytes 1572868
  197.4 119.4 %copy-start.19 = (f32[2,2]{1,0:T(2,128)S(1)}, f32[2,2]{1,0:T(2,128)}, u32[]{:S(2)}) copy-start(f32[2,2]{1,0:T(2,128)} %param.38) | copy-start | bytes 52
  197.4 144.0 %copy-start.18 = (f32[2,2,128]{2,1,0:T(2,128)S(1)}, f32[2,2,128]{2,1,0:T(2,128)}, u32[]{:S(2)}) copy-start(f32[2,2,128]{2,1,0:T(2,128)} %param.37) | copy-start | bytes 6148
  255.6 93.8 %copy-start.9 = (f32[8,2,128,128]{3,2,1,0:T(8,128)S(1)}, f32[8,2,128,128]{3,2,1,0:T(8,128)}, u32[]{:S(2)}) copy-start(f32[8,2,128,128]{3,2,1,0:T(8,128)} %get-tuple-element.142) | copy-start | bytes 3145732
  259.1 94.1 %collective-permute-start = (bf16[8,128]{1,0:T(8,128)(2,1)S(1)}, bf16[8,128]{1,0:T(8,128)(2,1)S(1)}, u32[]{:S(2)}, u32[]{:S(2)}) collective-permute-start(bf16[8,128]{1,0:T(8,128)(2,1)S(1)} %get-tuple-element.443), channel_id=1, source_target_pairs={{0,4},{4,8},{8,12},{12,16},{16,20},{20,24},{24,28},{28,32},{32,36}... | collective-permute-start | bytes 6152 | tf_op jit(solution)/shard_map/ppermute | solution.py:19
  263.0 90.2 %collective-permute-start.1 = (bf16[8,128]{1,0:T(8,128)(2,1)S(1)}, bf16[8,128]{1,0:T(8,128)(2,1)S(1)}, u32[]{:S(2)}, u32[]{:S(2)}) collective-permute-start(bf16[8,128]{1,0:T(8,128)(2,1)S(1)} %get-tuple-element.444), channel_id=1, source_target_pairs={{4,0},{8,4},{12,8},{16,12},{20,16},{24,20},{28,24},{32,28},{36,32}... | collective-permute-start | bytes 6152 | tf_op jit(solution)/shard_map/ppermute | solution.py:22
  344.4 8.8 %slice-start = ((bf16[1024,1152]{1,0:T(8,128)(2,1)}), bf16[1024,128]{1,0:T(8,128)(2,1)S(1)}, s32[]{:S(2)}) async-start(bf16[1024,1152]{1,0:T(8,128)(2,1)} %copy-done.10), calls=%async_computation.3 | async-start | bytes 524288 | tf_op jit(solution)/shard_map/slice | solution.py:194
  344.4 8.8 %copy-start.21 = (f32[128]{0:T(128)S(1)}, f32[128]{0:T(128)}, u32[]{:S(2)}) copy-start(f32[128]{0:T(128)} %dynamic_slice.60) | copy-start | bytes 1540
  355.4 5.5 %copy-start.8 = (bf16[2,1024,128]{2,1,0:T(8,128)(2,1)S(1)}, bf16[2,1024,128]{2,1,0:T(8,128)(2,1)}, u32[]{:S(2)}) copy-start(bf16[2,1024,128]{2,1,0:T(8,128)(2,1)} %copy-done.7) | copy-start | bytes 1572868
  355.4 5.5 %copy-start.14 = (f32[2,1024,128]{1,2,0:T(8,128)S(1)}, f32[2,1024,128]{1,2,0:T(8,128)}, u32[]{:S(2)}) copy-start(f32[2,1024,128]{1,2,0:T(8,128)} %reshape.668) | copy-start | bytes 3145732
  355.4 5.5 %copy-start.20 = (f32[2,2,128,128]{3,2,1,0:T(8,128)S(1)}, f32[2,2,128,128]{3,2,1,0:T(8,128)}, u32[]{:S(2)}) copy-start(f32[2,2,128,128]{3,2,1,0:T(8,128)} %param.36) | copy-start | bytes 786436
  360.9 13.6 %copy-start.5 = (bf16[128,2,8,128]{3,2,1,0:T(8,128)(2,1)S(1)}, bf16[128,2,8,128]{3,2,1,0:T(8,128)(2,1)}, u32[]{:S(2)}) copy-start(bf16[128,2,8,128]{3,2,1,0:T(8,128)(2,1)} %copy-done.4) | copy-start | bytes 1572868
Sparse Core Ops, SparseCore 0:
  9.0 51.1 all-gather.9
  256.4 47.1 all-gather.11
